TPU v7x, 512 devices: a whole 4x8x8 slice. The times are simulated.
512 devices in a mesh: ep: 32 (over z, x), tp: 16 (over y, core).
Axes of the slice: x: 4, y: 8, z: 8, core: 2. Of those that a mesh axis runs over, the one named last changes fastest.
Arguments:
- mixer_query: bfloat16 [8192, 2048], P('ep', 'tp'), may hold values from -6 to 6
- mixer_forget: bfloat16 [8192, 2048], P('ep', 'tp'), may hold values from -5.5 to 5.5
- mixer_value: bfloat16 [8192, 2048], P('ep', 'tp'), may hold values from -6 to 6
- mixer_gate: bfloat16 [8192, 2048], P('ep', 'tp'), may hold values from -6 to 6
- forget_floor: float32 [2048], P('tp'), may hold values from 0.88 to 1
- head_gain: float32 [128], replicated, may hold values from 0.1 to 1.9
- mixer_proj: bfloat16 [2048, 2048], P(None, 'tp'), may hold values from -0.125 to 0.125
- expert_tokens: bfloat16 [4096, 2048], P('ep'), may hold values from -6 to 6
- expert_gain: float32 [2048], replicated, may hold values from 0.1 to 1.9
- routes: int32 [4096, 2], P('ep'), may hold values from 0 to 31, as said below
- group_logits: float32 [4096, 4], P('ep'), may hold values from -6 to 6
- choice_logits: float32 [4096, 2], P('ep'), may hold values from -6 to 6
- w_gate: bfloat16 [32, 2048, 2048], P('ep', None, 'tp'), may hold values from -0.125 to 0.125
- w_up: bfloat16 [32, 2048, 2048], P('ep', None, 'tp'), may hold values from -0.125 to 0.125
- w_down: bfloat16 [32, 2048, 2048], P('ep', None, 'tp'), may hold values from -0.125 to 0.125
Outputs:
- mixer_out: bfloat16 [8192, 2048], P('ep', 'tp')
- expert_out: bfloat16 [4096, 2048], P('ep', 'tp')
Inputs may be any that keep to these rules, and one draw needn't show every extreme that they name: `routes`: in each aligned block of 128 rows (the rows of one index of ep) no expert is named by more than 16 rows, and some expert reaches that bound in every block; the 2 experts of a row differ and lie in the same group.
All inputs are finite; a program needn't handle non-finite values.
Results may differ from a plain program's by a relative error of at most 0.01.
Values may be sent and summed in bfloat16 or wider, within the bound.
A program may use at most 64 MiB of HBM per device.

v0:
```python
import jax
import jax.numpy as jnp
from jax import lax
from jax.sharding import Mesh
from jax.sharding import PartitionSpec as P

KEYDIM = 128
VDIM = 128
GROUPS = 4
TOPK = 2
BLOCK = 64
EP = ("ep_0", "ep_1")
norm_eps = 1e-06
highest_precision = lax.Precision.HIGHEST


def filled_with(shard, identity):
    return jax.tree.map(
        lambda part, zero: jnp.zeros_like(part) + jnp.asarray(zero, part.dtype), shard, identity
    )


def collected_together(shard, axis):
    leaves = jax.tree.leaves(shard)
    sequence = sorted(range(len(leaves)), key=lambda k: -leaves[k].size)
    width = (1, *leaves[sequence[0]].shape)[-1]
    lines = [
        jnp.pad(leaves[k].reshape(-1), (0, -leaves[k].size % width)).reshape(-1, width)
        for k in sequence
    ]
    both, at, found = (lax.all_gather(jnp.concatenate(lines), axis), 0, {})
    for k, line in zip(sequence, lines):
        section = both[:, at : at + len(line)].reshape(len(both), -1)
        found[k] = section[:, : leaves[k].size].reshape(-1, *leaves[k].shape)
        at += len(line)
    numbers = iter(range(len(leaves)))
    return jax.tree.map(lambda _: found[next(numbers)], shard)


def carried_in(shard, axes, combine, identity):
    before = start = filled_with(shard, identity)
    so_far = shard
    for axis in reversed(axes):
        devices, index = (lax.axis_size(axis), lax.axis_index(axis))
        pieces = collected_together(
            jax.tree.map(
                lambda part, kind: part.astype(kind), so_far, (jnp.bfloat16, jnp.bfloat16)
            ),
            axis,
        )
        inside, so_far = (start, start)
        for k in range(devices):
            passed = k < index
            so_far = combine(
                so_far, jax.tree.map(lambda part, own: part[k].astype(own.dtype), pieces, shard)
            )
            inside = jax.tree.map(lambda new, old: jnp.where(passed, new, old), so_far, inside)
        before = combine(inside, before)
    return before


def laid_out(pieces, dim):
    dims = list(pieces.shape[1:])
    dims[dim] *= pieces.shape[0]
    return jnp.moveaxis(pieces, 0, dim).reshape(dims)


def from_everyone(shard, axis):
    copies = jnp.broadcast_to(shard, (lax.axis_size(axis), *shard.shape))
    return lax.all_to_all(copies, axis, split_axis=0, concat_axis=0, tiled=True)


def gather_directly(shard, axis, dim):
    return laid_out(from_everyone(shard, axis), dim)


def rms_scale(features, gain_vec):
    return (
        features
        * lax.rsqrt(jnp.mean(features * features, axis=-1, keepdims=True) + norm_eps)
        * gain_vec
    )


def block_terms(query_block, input_block, log_blk, value_block, carried_state):
    cumulative_log = jnp.cumsum(log_blk, axis=0)
    between_block_term = jnp.einsum(
        "zug,ugr->zur",
        query_block * jnp.exp(cumulative_log),
        carried_state,
        precision=highest_precision,
    )
    causal = jnp.tril(jnp.ones((query_block.shape[0], query_block.shape[0]), dtype=bool))[
        :, :, None, None
    ]
    differ = cumulative_log[:, None] - cumulative_log[None, :]
    decays = jnp.exp(jnp.where(causal, differ, -jnp.inf))
    scores = jnp.sum(query_block[:, None] * input_block[None, :] * decays, axis=-1)
    result = between_block_term + jnp.einsum(
        "tsh,shv->thv", scores, value_block, precision=highest_precision
    )
    ending_log_decay = cumulative_log[-1]
    updated_state = jnp.exp(ending_log_decay)[..., None] * carried_state + jnp.einsum(
        "twa,twr->war",
        input_block * jnp.exp(ending_log_decay[None] - cumulative_log),
        value_block,
        precision=highest_precision,
    )
    return (updated_state, result, cumulative_log)


def mixer_local(
    mixer_query, mixer_forget, mixer_value, mixer_gate, forget_floor, head_gain, mixer_proj
):
    length = mixer_query.shape[0]
    heads_local = mixer_query.shape[1] // KEYDIM
    blocks = length // BLOCK

    def split_blocks(source_array, last_width):
        return source_array.reshape(blocks, BLOCK, heads_local, last_width)

    queries = jax.nn.silu(mixer_query.astype(jnp.float32))
    input_rates = (1.0 - forget_floor) * jax.nn.sigmoid(-mixer_forget.astype(jnp.float32))
    log_forget = jnp.log1p(-input_rates)
    value_rows = mixer_value.astype(jnp.float32)

    def advance(carry_pair, block_inputs):
        carried_state, offset_log = carry_pair
        query_block, input_block, value_block, log_blk = block_inputs
        updated_state, result, cumulative_log = block_terms(
            query_block, input_block, log_blk, value_block, carried_state
        )
        scaled_values = query_block * jnp.exp(cumulative_log + offset_log[None])
        return ((updated_state, offset_log + cumulative_log[-1]), (result, scaled_values))

    initial = (
        jnp.zeros((heads_local, KEYDIM, VDIM), jnp.float32),
        jnp.zeros((heads_local, KEYDIM), jnp.float32),
    )
    (local_state, total_log), (output_rows, scaled_values) = lax.scan(
        advance,
        initial,
        (
            split_blocks(queries, KEYDIM),
            split_blocks(input_rates, KEYDIM),
            split_blocks(value_rows, VDIM),
            split_blocks(log_forget, KEYDIM),
        ),
    )

    def combine(earlier, later):
        return (earlier[0] * later[0], later[0][..., None] * earlier[1] + later[1])

    identity = (jnp.ones_like(total_log), jnp.zeros_like(local_state))
    incoming_state = carried_in((jnp.exp(total_log), local_state), EP, combine, identity)
    output_rows = output_rows + jnp.einsum(
        "qsfa,fap->qsfp", scaled_values, incoming_state[1], precision=highest_precision
    )
    output_rows = output_rows.reshape(length, heads_local, VDIM)
    gate_act = jax.nn.silu(mixer_gate.astype(jnp.float32)).reshape(length, heads_local, VDIM)
    gated_out = rms_scale(output_rows, head_gain) * gate_act
    mixed_heads = gated_out.reshape(length, heads_local * VDIM).astype(jnp.bfloat16)
    summed = jnp.dot(
        lax.all_gather(mixed_heads, "tp", axis=1, tiled=True),
        mixer_proj,
        preferred_element_type=jnp.float32,
    )
    return summed.astype(jnp.bfloat16)


def gate_weights(routes, group_logits, choice_logits, group_size):
    group_exp = jnp.exp(group_logits)
    group_prob = group_exp / jnp.sum(group_exp, axis=-1, keepdims=True)
    groups_of = routes // group_size
    member = (groups_of[..., None] == jnp.arange(GROUPS, dtype=jnp.int32)).astype(jnp.float32)
    picked_prob = jnp.sum(member * group_prob[:, None, :], axis=-1)
    choice_exp = jnp.exp(choice_logits)
    together = (groups_of[:, :, None] == groups_of[:, None, :]).astype(jnp.float32)
    within = jnp.sum(together * choice_exp[:, None, :], axis=-1)
    return picked_prob * choice_exp / within


def finish(gate_pre, up_pre, down_local, sources, slot_count):
    hidden = (jax.nn.silu(gate_pre) * up_pre).astype(jnp.bfloat16)
    summed = jnp.dot(
        gather_directly(hidden, "tp", 1), down_local, preferred_element_type=jnp.float32
    )
    shaped = summed.astype(jnp.bfloat16).reshape(sources, slot_count, down_local.shape[1])
    return lax.all_to_all(shaped, EP, split_axis=0, concat_axis=0, tiled=True)


def expert_local(
    expert_tokens, expert_gain, routes, group_logits, choice_logits, w_gate, w_up, w_down
):
    count_rows, model_width = expert_tokens.shape
    experts_all = lax.axis_size(EP)
    capacity = 2 * TOPK * count_rows // experts_all
    normed = rms_scale(expert_tokens.astype(jnp.float32), expert_gain).astype(jnp.bfloat16)
    weights = gate_weights(routes, group_logits, choice_logits, experts_all // GROUPS)
    flat_routes = routes.reshape(-1)
    onehot = (flat_routes[:, None] == jnp.arange(experts_all, dtype=jnp.int32)).astype(jnp.int32)
    earlier = jnp.cumsum(onehot, axis=0) - onehot
    ranks = jnp.sum(earlier * onehot, axis=-1)
    slot_of = flat_routes * capacity + ranks
    token_ids = jnp.arange(flat_routes.shape[0], dtype=jnp.int32) // TOPK
    token_of = jnp.full((experts_all * capacity,), count_rows, jnp.int32).at[slot_of].set(token_ids)
    padded = jnp.concatenate([normed, jnp.zeros((1, model_width), jnp.bfloat16)], axis=0)
    outgoing = padded[token_of].reshape(experts_all, capacity, model_width)
    gate_local = w_gate[0]
    up_local = w_up[0]
    down_local = w_down[0]
    arrived = lax.all_to_all(outgoing, EP, split_axis=0, concat_axis=0, tiled=True)
    sources, slot_count, _ = arrived.shape
    flat_in = arrived.reshape(sources * slot_count, model_width)
    gate_pre = jnp.dot(flat_in, gate_local, preferred_element_type=jnp.float32)
    up_pre = jnp.dot(flat_in, up_local, preferred_element_type=jnp.float32)
    came_back = finish(gate_pre, up_pre, down_local, sources, slot_count)
    picked = (
        came_back.reshape(-1, came_back.shape[-1])[slot_of].astype(jnp.float32)
        * weights.reshape(-1)[:, None]
    )
    return jnp.sum(picked.reshape(count_rows, TOPK, -1), axis=1).astype(jnp.bfloat16)


def per_device(
    mixer_query,
    mixer_forget,
    mixer_value,
    mixer_gate,
    forget_floor,
    head_gain,
    mixer_proj,
    expert_tokens,
    expert_gain,
    routes,
    group_logits,
    choice_logits,
    w_gate,
    w_up,
    w_down,
):
    mixer_out = mixer_local(
        mixer_query, mixer_forget, mixer_value, mixer_gate, forget_floor, head_gain, mixer_proj
    )
    expert_out = expert_local(
        expert_tokens, expert_gain, routes, group_logits, choice_logits, w_gate, w_up, w_down
    )
    return (mixer_out, expert_out)


def solution(mesh):
    finer = Mesh(mesh.devices.reshape(8, 4, mesh.shape["tp"]), ("ep_0", "ep_1", "tp"))
    placed = (
        P(EP, "tp"),
        P(EP, "tp"),
        P(EP, "tp"),
        P(EP, "tp"),
        P("tp"),
        P(),
        P(None, "tp"),
        P(EP, None),
        P(),
        P(EP, None),
        P(EP, None),
        P(EP, None),
        P(EP, None, "tp"),
        P(EP, None, "tp"),
        P(EP, None, "tp"),
    )
    return jax.shard_map(
        per_device,
        mesh=finer,
        in_specs=placed,
        out_specs=(P(EP, "tp"), P(EP, "tp")),
        check_vma=False,
    )
```

profile of v0, /device:TPU:1, one launch (start us, length us, event | category | flops | bytes accessed | tf_op | source)
XLA Modules:
  0.0 173.8 jit_solution(17011988294751444505)
XLA Ops:
  7.2 0.8 copy.50
  10.2 1.4 scatter_custom_fusion
  11.6 1.2 fusion.24
  12.9 1.2 fusion.26
  14.2 3.3 %gather_fusion = bf16[512,2048]{1,0:T(8,128)(2,1)} fusion(bf16[129,2048]{1,0:T(8,128)(2,1)S(1)} %concatenate.11, s32[1024]{0:T(1024)S(1)} %pad_clamp_fusion.1), kind=kCustom, calls=%fused_computation | custom fusion | bytes 4196352 | tf_op jit(solution)/shard_map/gather | solution.py:208
  17.5 13.8 %all-to-all-start = ((bf16[32,16,2048]{2,1,0:T(8,128)(2,1)}), bf16[32,16,2048]{2,1,0:T(8,128)(2,1)S(1)}, u32[]{:S(2)}, u32[]{:S(2)}) async-start(bf16[32,16,2048]{2,1,0:T(8,128)(2,1)} %bitcast.31), calls=%async_computation | async-start | bytes 4194304 | tf_op jit(solution)/shard_map/all_to_all | solution.py:212
  31.6 13.7 %while.17 = (s32[]{:T(128)}, f32[1,128,128]{2,1,0:T(8,128)S(1)}, f32[1,128]{1,0:T(1,128)S(1)}, f32[4,64,1,128]{3,1,2,0:T(8,128)}, f32[4,64,1,128]{3,1,2,0:T(8,12...) while((s32[]{:T(128)}, f32[1,128,128]{2,1,0:T(8,128)S(1)}, ...), condition=%wide.region_3.4_spmd.clone, body=%wide.region_0.3_spmd.clone.sunk | while | flops 34709760 | bytes 1030797 | solution.py:140
  32.4 1.4 multiply_reduce_fusion.3
  35.8 1.4 multiply_reduce_fusion.3
  39.2 1.4 multiply_reduce_fusion.3
  42.7 1.4 multiply_reduce_fusion.3
  45.4 10.6 %all-gather.2 = bf16[4,129,128]{2,1,0:T(8,128)(2,1)S(1)} all-gather(bf16[1,129,128]{2,1,0:T(8,128)(2,1)S(1)} %maximum_bitcast_fusion), channel_id=2, replica_groups=mesh['ep_0'=8,'ep_1'=4,'tp'=16] {'ep_1'}, dimensions={0}, use_global_device_ids=true | all-gather | bytes 165120 | tf_op jit(solution)/shard_map/all_gather | solution.py:31
  56.0 23.8 %all-to-all-done = bf16[32,16,2048]{2,1,0:T(8,128)(2,1)S(1)} async-done(((bf16[32,16,2048]{2,1,0:T(8,128)(2,1)}), bf16[32,16,2048]{2,1,0:T(8,128)(2,1)S(1)}, u32[]{:S(2)}, u32[]{:S(2)}) %all-to-all-start) | async-done | bytes 2097184 | tf_op jit(solution)/shard_map/all_to_all | solution.py:212
  81.4 1.6 broadcast_in_dim.37
  83.0 9.9 %all-to-all-start.1 = ((bf16[16,512,128]{1,2,0:T(8,128)(2,1)}), bf16[16,512,128]{1,2,0:T(8,128)(2,1)S(1)}, u32[]{:S(2)}, u32[]{:S(2)}) async-start(bf16[16,512,128]{1,2,0:T(8,128)(2,1)} %broadcast_in_dim.37), calls=%async_computation.1 | async-start | bytes 4194304 | tf_op jit(solution)/shard_map/all_to_all | solution.py:70
  93.1 20.6 %all-gather.3 = bf16[8,129,128]{2,1,0:T(8,128)(2,1)S(1)} all-gather(bf16[1,129,128]{2,1,0:T(8,128)(2,1)S(1)} %maximum_bitcast_fusion.1), channel_id=3, replica_groups=mesh['ep_0'=8,'ep_1'=4,'tp'=16] {'ep_0'}, dimensions={0}, use_global_device_ids=true | all-gather | bytes 297216 | tf_op jit(solution)/shard_map/all_gather | solution.py:31
  113.8 1.7 multiply_reduce_fusion.1
  116.6 26.2 %all-to-all-done.1 = bf16[16,512,128]{1,2,0:T(8,128)(2,1)S(1)} async-done(((bf16[16,512,128]{1,2,0:T(8,128)(2,1)}), bf16[16,512,128]{1,2,0:T(8,128)(2,1)S(1)}, u32[]{:S(2)}, u32[]{:S(2)}) %all-to-all-start.1) | async-done | bytes 2097184 | tf_op jit(solution)/shard_map/all_to_all | solution.py:70
  142.8 2.4 %convolution_convert_fusion = bf16[512,128]{1,0:T(8,128)(2,1)} fusion(bf16[512,2048]{0,1:T(8,128)(2,1)S(1)} %bitcast.225, bf16[1,2048,128]{2,1,0:T(8,128)(2,1)} %param.31), kind=kOutput, calls=%fused_computation.42 | convolution fusion | flops 268500992 | bytes 2752512 | tf_op jit(solution)/shard_map/dot_general | solution.py:185
  145.2 5.1 %all-to-all-start.2 = ((bf16[32,16,128]{2,1,0:T(8,128)(2,1)}), bf16[32,16,128]{2,1,0:T(8,128)(2,1)S(1)}, u32[]{:S(2)}, u32[]{:S(2)}) async-start(bf16[32,16,128]{2,1,0:T(8,128)(2,1)} %bitcast.38), calls=%async_computation.2 | async-start | bytes 262144 | tf_op jit(solution)/shard_map/all_to_all | solution.py:189
  150.3 12.6 %all-gather.6.cloned.1.call-done = bf16[256,2048]{1,0:T(8,128)(2,1)} async-done(((bf16[256,128]{1,0:T(8,128)(2,1)}), bf16[256,2048]{1,0:T(8,128)(2,1)}) %all-gather.6.cloned.1.call-update) | async-done | bytes 1048592 | tf_op jit(solution)/shard_map/all_gather | solution.py:164
  162.9 2.3 %convolution_convert_fusion.1 = bf16[256,128]{1,0:T(8,128)(2,1)} fusion(bf16[256,2048]{1,0:T(8,128)(2,1)} %all-gather.6.cloned.1.call-done, bf16[2048,128]{1,0:T(8,128)(2,1)S(1)} %copy-done.1), kind=kOutput, calls=%fused_computation.45 | convolution fusion | flops 134250496 | bytes 1638400 | tf_op jit(solution)/shard_map/dot_general | solution.py:163
  165.2 0.9 gather_fusion.1
  166.1 0.9 fusion.38
  (122 shorter events, 13.3 us)
Async XLA Ops:
  7.2 72.7 %copy-start = (bf16[1,2048,128]{2,1,0:T(8,128)(2,1)S(1)}, bf16[1,2048,128]{2,1,0:T(8,128)(2,1)}, u32[]{:S(2)}) copy-start(bf16[1,2048,128]{2,1,0:T(8,128)(2,1)} %param.29) | copy-start | bytes 1572868
  17.5 13.9 %copy-start.10 = (f32[128]{0:T(128)S(1)}, f32[128]{0:T(128)}, u32[]{:S(2)}) copy-start(f32[128]{0:T(128)} %param.21) | copy-start | bytes 1540
  17.5 13.9 %copy-start.2 = (bf16[256,128]{1,0:T(8,128)(2,1)S(1)}, bf16[256,128]{1,0:T(8,128)(2,1)}, u32[]{:S(2)}) copy-start(bf16[256,128]{1,0:T(8,128)(2,1)} %param.19) | copy-start | bytes 196612
  17.5 14.0 %copy-start.3 = (bf16[256,128]{1,0:T(8,128)(2,1)S(1)}, bf16[256,128]{1,0:T(8,128)(2,1)}, u32[]{:S(2)}) copy-start(bf16[256,128]{1,0:T(8,128)(2,1)} %param.17) | copy-start | bytes 196612
  17.5 14.0 %copy-start.4 = (bf16[256,128]{1,0:T(8,128)(2,1)S(1)}, bf16[256,128]{1,0:T(8,128)(2,1)}, u32[]{:S(2)}) copy-start(bf16[256,128]{1,0:T(8,128)(2,1)} %param.18) | copy-start | bytes 196612
  17.5 62.3 %all-to-all-start = ((bf16[32,16,2048]{2,1,0:T(8,128)(2,1)}), bf16[32,16,2048]{2,1,0:T(8,128)(2,1)S(1)}, u32[]{:S(2)}, u32[]{:S(2)}) async-start(bf16[32,16,2048]{2,1,0:T(8,128)(2,1)} %bitcast.31), calls=%async_computation | async-start | bytes 4194304 | tf_op jit(solution)/shard_map/all_to_all | solution.py:212
  45.4 35.2 %copy-start.9 = (bf16[1,2048,128]{2,1,0:T(8,128)(2,1)S(1)}, bf16[1,2048,128]{2,1,0:T(8,128)(2,1)}, u32[]{:S(2)}) copy-start(bf16[1,2048,128]{2,1,0:T(8,128)(2,1)} %param.30) | copy-start | bytes 1572868
  83.0 32.6 %copy-start.5 = (bf16[256,128]{1,0:T(8,128)(2,1)S(1)}, bf16[256,128]{1,0:T(8,128)(2,1)}, u32[]{:S(2)}) copy-start(bf16[256,128]{1,0:T(8,128)(2,1)} %param.20) | copy-start | bytes 196612
  83.0 32.6 %copy-start.8 = (f32[128]{0:T(128)S(1)}, f32[128]{0:T(128)}, u32[]{:S(2)}) copy-start(f32[128]{0:T(128)} %param.22) | copy-start | bytes 1540
  83.0 59.8 %all-to-all-start.1 = ((bf16[16,512,128]{1,2,0:T(8,128)(2,1)}), bf16[16,512,128]{1,2,0:T(8,128)(2,1)S(1)}, u32[]{:S(2)}, u32[]{:S(2)}) async-start(bf16[16,512,128]{1,2,0:T(8,128)(2,1)} %broadcast_in_dim.37), calls=%async_computation.1 | async-start | bytes 4194304 | tf_op jit(solution)/shard_map/all_to_all | solution.py:70
  92.9 23.5 %copy-start.7 = (f32[128,2]{0,1:T(2,128)S(1)}, f32[128,2]{0,1:T(2,128)}, u32[]{:S(2)}) copy-start(f32[128,2]{0,1:T(2,128)} %param.28) | copy-start | bytes 3076
  92.9 23.5 %copy-start.6 = (f32[128,4]{0,1:T(4,128)S(1)}, f32[128,4]{0,1:T(4,128)}, u32[]{:S(2)}) copy-start(f32[128,4]{0,1:T(4,128)} %param.27) | copy-start | bytes 6148
  92.9 70.0 %all-gather.6.cloned.1.call-start = ((), (), s32[]{:S(2)}) async-start(), calls=%async_computation.3 | async-start | bytes 1114112 | tf_op jit(solution)/shard_map/all_gather | solution.py:164
  113.8 49.2 %copy-start.1 = (bf16[2048,128]{1,0:T(8,128)(2,1)S(1)}, bf16[2048,128]{1,0:T(8,128)(2,1)}, u32[]{:S(2)}) copy-start(bf16[2048,128]{1,0:T(8,128)(2,1)} %param.23) | copy-start | bytes 1572868
  145.2 20.0 %all-to-all-start.2 = ((bf16[32,16,128]{2,1,0:T(8,128)(2,1)}), bf16[32,16,128]{2,1,0:T(8,128)(2,1)S(1)}, u32[]{:S(2)}, u32[]{:S(2)}) async-start(bf16[32,16,128]{2,1,0:T(8,128)(2,1)} %bitcast.38), calls=%async_computation.2 | async-start | bytes 262144 | tf_op jit(solution)/shard_map/all_to_all | solution.py:189
Sparse Core Ops, SparseCore 0:
  116.4 46.4 all-gather.5
where the time goes:
time: 174 us
  waiting for transfers between devices  62.6 us (36%)
  blocking collectives  31.2 us (18%)
  starting transfers between devices  28.9 us (17%)
  between operations  14.4 us (8%)
  other arithmetic  14.2 us (8%)
  matrix products  12.9 us (7%)
  local copies, waits for them, and re-layouts  9.24 us (5%)
    all_gather x2, blocking collectives, collected_together(): both, at, found = (lax.all_gather(jnp.concatenate(lines), axis), 0, {})  31.2 us
    all_to_all x1, waiting for transfers between devices, from_everyone(): return lax.all_to_all(copies, axis, split_axis=0, concat_axis=0, tiled=True)  26.2 us
    all_to_all x1, waiting for transfers between devices, expert_local(): lax.all_to_all(outgoing, EP, split_axis=0, concat_axis=0, tiled=True)  23.8 us
    all_to_all x1, starting transfers between devices, expert_local(): lax.all_to_all(outgoing, EP, split_axis=0, concat_axis=0, tiled=True)  13.8 us
    all_gather x1, waiting for transfers between devices, mixer_local(): lax.all_gather(mixed_heads, 'tp', axis=1, tiled=True)  12.6 us
    all_to_all x1, starting transfers between devices, from_everyone(): return lax.all_to_all(copies, axis, split_axis=0, concat_axis=0, tiled=True)  9.89 us
    reduce_sum x4, other arithmetic, block_terms(): jnp.sum(query_block[:, None] * input_block[None, :] * decays, axis=-1)  5.4 us
    all_to_all x1, starting transfers between devices, finish(): return lax.all_to_all(shaped, EP, split_axis=0, concat_axis=0, tiled=True)  5.08 us
  transfers between devices with their start and end apart: 4, of which 3 were waited for; matrix products, arithmetic and copies ran while one was open for 12% of the time, Pallas kernels for 0%

commit v1 on v0

--- a/solution.py
+++ b/solution.py
@@ -161,7 +161,7 @@
     gated_out = rms_scale(output_rows, head_gain) * gate_act
     mixed_heads = gated_out.reshape(length, heads_local * VDIM).astype(jnp.bfloat16)
     summed = jnp.dot(
-        lax.all_gather(mixed_heads, "tp", axis=1, tiled=True),
+        jnp.concatenate(lax.all_gather(mixed_heads, "tp"), axis=1),
         mixer_proj,
         preferred_element_type=jnp.float32,
     )

time: 174 us -> 193 us (1.11)
  waiting for transfers between devices: 62.6 us -> 78.4 us
  matrix products: 12.9 us -> 9.47 us
  blocking collectives: 31.2 us -> 34.6 us
  local copies, waits for them, and re-layouts: 9.24 us -> 11.9 us
  starting transfers between devices: 28.9 us -> 31.5 us
  other arithmetic: 14.2 us -> 11.7 us
    all_gather x1, waiting for transfers between devices: 12.6 us -> 46.1 us  [mixer_local(): lax.all_gather(mixed_heads, 'tp')]
    all_to_all x1, waiting for transfers between devices: 26.2 us -> 0.01 us  [from_everyone(): return lax.all_to_all(copies, axis, split_axis=0, concat_axis=0, tiled=True)]
    all_to_all x1, waiting for transfers between devices: 0.01 us -> 7.1 us  [finish(): return lax.all_to_all(shaped, EP, split_axis=0, concat_axis=0, tiled=True)]
    all_gather x2, blocking collectives: 31.2 us -> 34.6 us  [collected_together(): both, at, found = (lax.all_gather(jnp.concatenate(lines), axis), 0, {})]
    all_to_all x1, starting transfers between devices: 5.08 us -> 7.7 us  [finish(): return lax.all_to_all(shaped, EP, split_axis=0, concat_axis=0, tiled=True)]
    dot_general x4, matrix products: 3.09 us -> 0.67 us  [block_terms(): jnp.einsum('tsh,shv->thv', scores, value_block, precision=highest_precision)]
    dynamic_update_slice x4, other arithmetic: 2.49 us -> 0.08 us  [mixer_local(): lax.scan(advance, initial, (split_blocks(queries, KEYDIM), split_blocks(i...]
    reshape x0 -> x1, local copies, waits for them, and re-layouts: none -> 2.34 us  [mixer_local(): jnp.concatenate(lax.all_gather(mixed_heads, 'tp'), axis=1)]
  transfers between devices with their start and end apart: 4 -> 4, of which waited for: 3 -> 3; matrix products, arithmetic and copies ran while one was open for 12% -> 8% of each run, Pallas kernels for 0% -> 0%
where the time goes in v1:
time: 193 us; the launch traced here: 192 us
  waiting for transfers between devices  78.4 us (41%)
  blocking collectives  34.6 us (18%)
  starting transfers between devices  31.5 us (16%)
  between operations  14.4 us (7%)
  local copies, waits for them, and re-layouts  11.9 us (6%)
  other arithmetic  11.7 us (6%)
  matrix products  9.47 us (5%)
    all_gather x1, waiting for transfers between devices, mixer_local(): lax.all_gather(mixed_heads, 'tp')  46.1 us
    all_gather x2, blocking collectives, collected_together(): both, at, found = (lax.all_gather(jnp.concatenate(lines), axis), 0, {})  34.6 us
    all_to_all x1, waiting for transfers between devices, expert_local(): lax.all_to_all(outgoing, EP, split_axis=0, concat_axis=0, tiled=True)  25.2 us
    all_to_all x1, starting transfers between devices, expert_local(): lax.all_to_all(outgoing, EP, split_axis=0, concat_axis=0, tiled=True)  13.8 us
    all_to_all x1, starting transfers between devices, from_everyone(): return lax.all_to_all(copies, axis, split_axis=0, concat_axis=0, tiled=True)  9.89 us
    all_to_all x1, starting transfers between devices, finish(): return lax.all_to_all(shaped, EP, split_axis=0, concat_axis=0, tiled=True)  7.7 us
    all_to_all x1, waiting for transfers between devices, finish(): return lax.all_to_all(shaped, EP, split_axis=0, concat_axis=0, tiled=True)  7.1 us
    reduce_sum x4, other arithmetic, block_terms(): jnp.sum(query_block[:, None] * input_block[None, :] * decays, axis=-1)  5.33 us
  transfers between devices with their start and end apart: 4, of which 3 were waited for; matrix products, arithmetic and copies ran while one was open for 8% of the time, Pallas kernels for 0%

profile of v1, /device:TPU:1, one launch (start us, length us, event | category | flops | bytes accessed | tf_op | source)
XLA Modules:
  0.0 192.4 jit_solution(7422716623838126194)
XLA Ops:
  7.2 0.8 copy.74
  10.2 1.4 scatter_custom_fusion
  11.6 1.2 fusion.24
  12.9 1.2 fusion.26
  14.2 3.3 %gather_fusion = bf16[512,2048]{1,0:T(8,128)(2,1)} fusion(bf16[129,2048]{1,0:T(8,128)(2,1)S(1)} %concatenate.11, s32[1024]{0:T(1024)S(1)} %pad_clamp_fusion.1), kind=kCustom, calls=%fused_computation | custom fusion | bytes 4196352 | tf_op jit(solution)/shard_map/gather | solution.py:208
  17.5 13.8 %all-to-all-start = ((bf16[32,16,2048]{2,1,0:T(8,128)(2,1)}), bf16[32,16,2048]{2,1,0:T(8,128)(2,1)S(1)}, u32[]{:S(2)}, u32[]{:S(2)}) async-start(bf16[32,16,2048]{2,1,0:T(8,128)(2,1)} %bitcast.37), calls=%async_computation | async-start | bytes 4194304 | tf_op jit(solution)/shard_map/all_to_all | solution.py:212
  31.6 9.0 %while.17 = (s32[]{:T(128)}, f32[1,128,128]{2,1,0:T(8,128)S(1)}, f32[1,128]{1,0:T(1,128)S(1)}, f32[4,64,1,128]{3,1,2,0:T(8,128)S(1)}, f32[4,64,1,128]{3,1,2,0:T(...) while((s32[]{:T(128)}, f32[1,128,128]{2,1,0:T(8,128)S(1)}, ...), condition=%wide.region_3.4_spmd.clone, body=%wide.region_0.3_spmd.clone.sunk | while | flops 34709760 | bytes 1046165 | solution.py:140
  31.8 1.3 multiply_reduce_fusion.3
  34.1 1.3 multiply_reduce_fusion.3
  36.3 1.3 multiply_reduce_fusion.3
  38.5 1.3 multiply_reduce_fusion.3
  40.7 14.0 %all-gather.3 = bf16[4,129,128]{2,1,0:T(8,128)(2,1)S(1)} all-gather(bf16[1,129,128]{2,1,0:T(8,128)(2,1)S(1)} %maximum_bitcast_fusion), channel_id=2, replica_groups=mesh['ep_0'=8,'ep_1'=4,'tp'=16] {'ep_1'}, dimensions={0}, use_global_device_ids=true | all-gather | bytes 165120 | tf_op jit(solution)/shard_map/all_gather | solution.py:31
  54.7 25.2 %all-to-all-done = bf16[32,16,2048]{2,1,0:T(8,128)(2,1)S(1)} async-done(((bf16[32,16,2048]{2,1,0:T(8,128)(2,1)}), bf16[32,16,2048]{2,1,0:T(8,128)(2,1)S(1)}, u32[]{:S(2)}, u32[]{:S(2)}) %all-to-all-start) | async-done | bytes 2097184 | tf_op jit(solution)/shard_map/all_to_all | solution.py:212
  81.7 1.6 broadcast_in_dim.37
  83.3 9.9 %all-to-all-start.1 = ((bf16[16,512,128]{1,2,0:T(8,128)(2,1)}), bf16[16,512,128]{1,2,0:T(8,128)(2,1)S(1)}, u32[]{:S(2)}, u32[]{:S(2)}) async-start(bf16[16,512,128]{1,2,0:T(8,128)(2,1)} %broadcast_in_dim.37), calls=%async_computation.1 | async-start | bytes 4194304 | tf_op jit(solution)/shard_map/all_to_all | solution.py:70
  93.4 20.6 %all-gather.4 = bf16[8,129,128]{2,1,0:T(8,128)(2,1)S(1)} all-gather(bf16[1,129,128]{2,1,0:T(8,128)(2,1)S(1)} %maximum_bitcast_fusion.1), channel_id=3, replica_groups=mesh['ep_0'=8,'ep_1'=4,'tp'=16] {'ep_0'}, dimensions={0}, use_global_device_ids=true | all-gather | bytes 297216 | tf_op jit(solution)/shard_map/all_gather | solution.py:31
  115.8 46.1 %all-gather.7.cloned.1.call-done = bf16[4096,128]{1,0:T(8,128)(2,1)} async-done(((bf16[256,128]{1,0:T(8,128)(2,1)}), bf16[4096,128]{1,0:T(8,128)(2,1)}) %all-gather.7.cloned.1.call-update) | async-done | bytes 1048592 | tf_op jit(solution)/shard_map/all_gather | solution.py:164
  161.9 2.3 %copy.72 = bf16[256,16,128]{0,2,1:T(8,128)(2,1)} copy(bf16[256,16,128]{2,0,1:T(8,128)(2,1)} %bitcast.243) | data formatting | bytes 2097152 | tf_op jit(solution)/shard_map/reshape | solution.py:164
  164.2 2.4 %convolution_convert_fusion = bf16[512,128]{1,0:T(8,128)(2,1)} fusion(bf16[512,2048]{0,1:T(8,128)(2,1)S(1)} %bitcast.235, bf16[1,2048,128]{2,1,0:T(8,128)(2,1)} %param.31), kind=kOutput, calls=%fused_computation.42 | convolution fusion | flops 268500992 | bytes 2752512 | tf_op jit(solution)/shard_map/dot_general | solution.py:185
  166.7 7.7 %all-to-all-start.2 = ((bf16[32,16,128]{2,1,0:T(8,128)(2,1)}), bf16[32,16,128]{2,1,0:T(8,128)(2,1)S(1)}, u32[]{:S(2)}, u32[]{:S(2)}) async-start(bf16[32,16,128]{2,1,0:T(8,128)(2,1)} %bitcast.44), calls=%async_computation.2 | async-start | bytes 262144 | tf_op jit(solution)/shard_map/all_to_all | solution.py:189
  174.4 2.3 %convolution_convert_fusion.1 = bf16[256,128]{1,0:T(8,128)(2,1)} fusion(bf16[256,2048]{0,1:T(8,128)(2,1)} %bitcast.238, bf16[2048,128]{1,0:T(8,128)(2,1)S(1)} %copy-done.1), kind=kOutput, calls=%fused_computation.45 | convolution fusion | flops 134250496 | bytes 1638400 | tf_op jit(solution)/shard_map/dot_general | solution.py:163
  176.7 7.1 %all-to-all-done.2 = bf16[32,16,128]{2,1,0:T(8,128)(2,1)S(1)} async-done(((bf16[32,16,128]{2,1,0:T(8,128)(2,1)}), bf16[32,16,128]{2,1,0:T(8,128)(2,1)S(1)}, u32[]{:S(2)}, u32[]{:S(2)}) %all-to-all-start.2) | async-done | bytes 131104 | tf_op jit(solution)/shard_map/all_to_all | solution.py:189
  183.8 0.9 gather_fusion.1
  184.7 0.9 fusion.38
  (123 shorter events, 9.4 us)
Async XLA Ops:
  7.2 72.7 %copy-start = (bf16[1,2048,128]{2,1,0:T(8,128)(2,1)S(1)}, bf16[1,2048,128]{2,1,0:T(8,128)(2,1)}, u32[]{:S(2)}) copy-start(bf16[1,2048,128]{2,1,0:T(8,128)(2,1)} %param.29) | copy-start | bytes 1572868
  17.5 13.9 %copy-start.10 = (f32[128]{0:T(128)S(1)}, f32[128]{0:T(128)}, u32[]{:S(2)}) copy-start(f32[128]{0:T(128)} %param.21) | copy-start | bytes 1540
  17.5 13.9 %copy-start.2 = (bf16[256,128]{1,0:T(8,128)(2,1)S(1)}, bf16[256,128]{1,0:T(8,128)(2,1)}, u32[]{:S(2)}) copy-start(bf16[256,128]{1,0:T(8,128)(2,1)} %param.19) | copy-start | bytes 196612
  17.5 14.0 %copy-start.3 = (bf16[256,128]{1,0:T(8,128)(2,1)S(1)}, bf16[256,128]{1,0:T(8,128)(2,1)}, u32[]{:S(2)}) copy-start(bf16[256,128]{1,0:T(8,128)(2,1)} %param.17) | copy-start | bytes 196612
  17.5 14.0 %copy-start.4 = (bf16[256,128]{1,0:T(8,128)(2,1)S(1)}, bf16[256,128]{1,0:T(8,128)(2,1)}, u32[]{:S(2)}) copy-start(bf16[256,128]{1,0:T(8,128)(2,1)} %param.18) | copy-start | bytes 196612
  17.5 62.3 %all-to-all-start = ((bf16[32,16,2048]{2,1,0:T(8,128)(2,1)}), bf16[32,16,2048]{2,1,0:T(8,128)(2,1)S(1)}, u32[]{:S(2)}, u32[]{:S(2)}) async-start(bf16[32,16,2048]{2,1,0:T(8,128)(2,1)} %bitcast.37), calls=%async_computation | async-start | bytes 4194304 | tf_op jit(solution)/shard_map/all_to_all | solution.py:212
  79.9 1.0 copy-start.9
  83.3 31.5 %copy-start.5 = (bf16[256,128]{1,0:T(8,128)(2,1)S(1)}, bf16[256,128]{1,0:T(8,128)(2,1)}, u32[]{:S(2)}) copy-start(bf16[256,128]{1,0:T(8,128)(2,1)} %param.20) | copy-start | bytes 196612
  83.3 31.5 %copy-start.8 = (f32[128]{0:T(128)S(1)}, f32[128]{0:T(128)}, u32[]{:S(2)}) copy-start(f32[128]{0:T(128)} %param.22) | copy-start | bytes 1540
  83.3 80.9 %all-to-all-start.1 = ((bf16[16,512,128]{1,2,0:T(8,128)(2,1)}), bf16[16,512,128]{1,2,0:T(8,128)(2,1)S(1)}, u32[]{:S(2)}, u32[]{:S(2)}) async-start(bf16[16,512,128]{1,2,0:T(8,128)(2,1)} %broadcast_in_dim.37), calls=%async_computation.1 | async-start | bytes 4194304 | tf_op jit(solution)/shard_map/all_to_all | solution.py:70
  93.2 22.4 %copy-start.7 = (f32[128,2]{0,1:T(2,128)S(1)}, f32[128,2]{0,1:T(2,128)}, u32[]{:S(2)}) copy-start(f32[128,2]{0,1:T(2,128)} %param.28) | copy-start | bytes 3076
  93.2 22.4 %copy-start.6 = (f32[128,4]{0,1:T(4,128)S(1)}, f32[128,4]{0,1:T(4,128)}, u32[]{:S(2)}) copy-start(f32[128,4]{0,1:T(4,128)} %param.27) | copy-start | bytes 6148
  93.2 68.7 %all-gather.7.cloned.1.call-start = ((), (), s32[]{:S(2)}) async-start(), calls=%async_computation.3 | async-start | bytes 1114112 | tf_op jit(solution)/shard_map/all_gather | solution.py:164
  161.9 12.5 %copy-start.1 = (bf16[2048,128]{1,0:T(8,128)(2,1)S(1)}, bf16[2048,128]{1,0:T(8,128)(2,1)}, u32[]{:S(2)}) copy-start(bf16[2048,128]{1,0:T(8,128)(2,1)} %param.23) | copy-start | bytes 1572868
  166.7 17.2 %all-to-all-start.2 = ((bf16[32,16,128]{2,1,0:T(8,128)(2,1)}), bf16[32,16,128]{2,1,0:T(8,128)(2,1)S(1)}, u32[]{:S(2)}, u32[]{:S(2)}) async-start(bf16[32,16,128]{2,1,0:T(8,128)(2,1)} %bitcast.44), calls=%async_computation.2 | async-start | bytes 262144 | tf_op jit(solution)/shard_map/all_to_all | solution.py:189
Sparse Core Ops, SparseCore 0:
  115.7 46.1 all-gather.6
